TPU v7x, 32 devices: a whole 2x2x4 slice. The times are simulated.
32 devices in a mesh: st: 16 (over z, y, x), tp: 2 (over core).
Axes of the slice: x: 2, y: 2, z: 4, core: 2. Of those that a mesh axis runs over, the one named last changes fastest.
Arguments:
- tokens: bfloat16 [12288, 2048], P('st'), may hold values from -6 to 6, as said below
- route_ids: int32 [192, 4], P('st'), may hold values from 0 to 383, as said below
- store: bfloat16 [384, 128, 2048], P('st'), may hold values from -6 to 6, as said below
- token_gain: float32 [2048], replicated, may hold values from 0.1 to 1.9
- store_gain: float32 [2048], replicated, may hold values from 0.1 to 1.9
- carry_weight: bfloat16 [2048, 512], P(None, 'tp'), may hold values from -0.125 to 0.125
- spatial_weight: bfloat16 [2048, 512], P(None, 'tp'), may hold values from -0.125 to 0.125
- spatial_gain: float32 [512], P('tp'), may hold values from 0.1 to 1.9
- position_mix: bfloat16 [8, 128, 128], P('tp'), may hold values from -0.5 to 0.5
- position_bias: float32 [8, 128], P('tp'), may hold values from 0.1 to 1.9
- query_weight: bfloat16 [2048, 512], P(None, 'tp'), may hold values from -0.86178639 to 0.86178639, as said below
- key_weight: bfloat16 [2048, 512], P(None, 'tp'), may hold values from -0.86178639 to 0.86178639, as said below
- read_weight: bfloat16 [2048, 512], P(None, 'tp'), may hold values from -0.125 to 0.125
- blend_weight: bfloat16 [2048, 512], P(None, 'tp'), may hold values from -0.125 to 0.125
- output_weight: bfloat16 [512, 2048], replicated, may hold values from -0.25 to 0.25
Outputs:
- mixed: bfloat16 [12288, 2048], P(('st', 'tp'))
Inputs may be any that keep to these rules, and one draw needn't show every extreme that they name: `route_ids`: each entry is a passage index; passage p is held by index p // 24 of st. All entries of the spans of one index of st (aligned blocks of 12 rows) are different; they name at most 6 passage held by any one index of st, exactly 6 held by the index before their own (cyclically), and at least one held by the index half the axis away. `tokens`: Activations; in some draws the first token of some spans equals a row of a passage that the span reads. `store`: passage rows. `query_weight`: A projection matrix. `key_weight`: A projection matrix.
All inputs are finite; a program needn't handle non-finite values.
Results may differ from a plain program's by a relative error of at most 0.012.
The roundings to bfloat16 on the way count: a program that leaves them out, or rounds other values in their place, can miss the bound.
Values may be sent and summed in bfloat16 or wider, within the bound.
No kernel may reach another device: no remote copies, remote signals or barrier semaphores. Data moves between devices by JAX's collectives and lax.ppermute only.
A program may use at most 128 MiB of HBM per device.

v0:
```python
import functools

import jax
import jax.numpy as jnp
from jax import lax
from jax.experimental import pallas as pl
from jax.experimental.pallas import tpu as pltpu
from jax.sharding import PartitionSpec as P

norm_eps = 1e-06
LANES = 128
LEVEL_TILE = 16
CHUNKS = 2
f32 = jnp.float32
bf16 = jnp.bfloat16


def params(semantics=None):
    return pltpu.CompilerParams(
        dimension_semantics=semantics, vmem_limit_bytes=56 * 1024 * 1024
    )


def rms_rows(values, gain):
    values = values.astype(f32)
    scale = lax.rsqrt(jnp.mean(values * values, axis=-1, keepdims=True) + norm_eps)
    return (values * scale * gain).astype(bf16)


def query_kernel(
    routes, tokens, gain, weight, normed, place, *rest, chunk_count, capacity, picks, span, held
):
    sent = rest[:chunk_count]
    queries, counts = rest[chunk_count:]
    step = pl.program_id(0)
    block = tokens.shape[0]
    rows = rms_rows(tokens[...], gain[...])
    normed[...] = rows
    start = pl.multiple_of(step * block, block)
    queries[pl.ds(start, block), :] = jnp.dot(
        rows, weight[...], preferred_element_type=f32
    ).astype(bf16)

    @pl.when(step == pl.num_programs(0) - 1)
    def _():
        owners = counts.shape[0]

        def clear(index, carry):
            counts[index] = 0
            return carry

        lax.fori_loop(0, owners, clear, 0)
        part = capacity // chunk_count

        def pack(request, carry):
            owner = lax.div(routes[request], held)
            rank = counts[owner]
            counts[owner] = rank + 1
            place[request] = owner * capacity + rank
            source = pl.multiple_of(lax.div(request, picks) * span, span)
            rows = queries[pl.ds(source, span), :]
            for chunk in range(chunk_count):

                @pl.when(lax.div(rank, part) == chunk)
                def _():
                    target = pl.multiple_of((rank - chunk * part) * span, span)
                    sent[chunk][owner, pl.ds(target, span), :] = rows

            return carry

        lax.fori_loop(0, routes.shape[0], pack, 0)


def store_kernel(store, gain, key_weight, read_weight, keys, values):
    count, length, width = store.shape
    rows = rms_rows(store[...].reshape(count * length, width), gain[...])
    found = jnp.dot(rows, key_weight[...], preferred_element_type=f32)
    keys[...] = found.astype(bf16).reshape(keys.shape)
    read = jnp.dot(rows, read_weight[...], preferred_element_type=f32)
    for index in range(count):
        values[index] = read[index * length : (index + 1) * length].T.astype(bf16)


def attend_kernel(local, queries, keys, values, out, *, part, span, head_dim):
    owners = queries.shape[0]
    width = queries.shape[2]
    pairs = width // LANES
    step = pl.program_id(0)
    scale = head_dim ** (-0.5)
    lane = lax.broadcasted_iota(jnp.int32, (span, LANES), 1)
    low = lane < head_dim
    level_row = lax.broadcasted_iota(jnp.int32, (LEVEL_TILE, LANES), 0)

    def one_owner(owner, carry):
        levels = [jnp.zeros((LEVEL_TILE, LANES), f32) for _ in range(pairs)]
        for slot in range(part):
            held = local[(step * owners + owner) * part + slot]
            for pair in range(pairs):
                cut = slice(pair * LANES, (pair + 1) * LANES)
                piece = queries[owner, slot * span : (slot + 1) * span, cut]
                zero = jnp.zeros_like(piece)
                both = jnp.concatenate(
                    [jnp.where(low, piece, zero), jnp.where(low, zero, piece)], axis=0
                )
                scores = (
                    lax.dot_general(
                        keys[held, :, cut],
                        both,
                        (((1,), (1,)), ((), ())),
                        preferred_element_type=f32,
                    )
                    * scale
                )
                peak = jnp.max(scores, axis=0, keepdims=True)
                weights = jnp.exp(scores - peak)
                total = jnp.sum(weights, axis=0, keepdims=True)
                summed = jnp.dot(
                    values[held, cut, :], weights.astype(bf16), preferred_element_type=f32
                )
                summed = jnp.where(low, summed[:head_dim], summed[head_dim:])
                out[owner, slot * span : (slot + 1) * span, cut] = (summed / total).astype(bf16)
                level = peak + jnp.log(total)
                first = level.astype(bf16).astype(f32)
                second = (level - first).astype(bf16).astype(f32)
                third = level - first - second
                for offset, row in enumerate((first, second, third)):
                    levels[pair] = jnp.where(
                        level_row == 3 * slot + offset, row, levels[pair]
                    )
        for pair in range(pairs):
            cut = slice(pair * LANES, (pair + 1) * LANES)
            out[owner, part * span : part * span + LEVEL_TILE, cut] = levels[pair].astype(bf16)
        return carry

    lax.fori_loop(0, owners, one_owner, 0)


def mixing_kernel(spatial, moments, gain, mix, bias, carry, out, *, head_dim, total_width):
    pairs = spatial.shape[1] // LANES
    mean = moments[:, 0:1] / total_width
    spread = moments[:, 1:2] / total_width - mean * mean
    rows = ((spatial[...] - mean) * lax.rsqrt(spread + norm_eps) * gain[...]).astype(bf16)
    lane = lax.broadcasted_iota(jnp.int32, (spatial.shape[0], LANES), 1)
    for pair in range(pairs):
        cut = slice(pair * LANES, (pair + 1) * LANES)
        first = jnp.dot(mix[2 * pair], rows[:, cut], preferred_element_type=f32)
        second = jnp.dot(mix[2 * pair + 1], rows[:, cut], preferred_element_type=f32)
        first = first + bias[:, 2 * pair : 2 * pair + 1]
        second = second + bias[:, 2 * pair + 1 : 2 * pair + 2]
        out[:, cut] = carry[:, cut] * jnp.where(lane < head_dim, first, second)


def merge_kernel(
    place, core, gated, gate, *rest, chunk_count, capacity, picks, span, head_dim
):
    back = rest[:chunk_count]
    keep, send = rest[chunk_count:]
    part = capacity // chunk_count
    spans = gated.shape[0] // span
    width = gated.shape[1]
    half = spans // 2
    lane = lax.broadcasted_iota(jnp.int32, (span, LANES), 1)
    low = lane < head_dim
    level_row = lax.broadcasted_iota(jnp.int32, (LEVEL_TILE, width), 0)

    def one_span(index, carry):
        levels = []
        pieces = []
        for pick in range(picks):
            at = place[index * picks + pick]
            owner = lax.div(at, capacity)
            rank = lax.rem(at, capacity)
            chunk = lax.div(rank, part)
            slot = rank - chunk * part
            source = pl.multiple_of(slot * span, span)
            piece = back[0][owner, pl.ds(source, span), :]
            tile = back[0][owner, part * span : part * span + LEVEL_TILE, :]
            piece = piece.astype(f32)
            tile = tile.astype(f32)
            for other in range(1, chunk_count):
                here = chunk == other
                piece = jnp.where(
                    here, back[other][owner, pl.ds(source, span), :].astype(f32), piece
                )
                tile = jnp.where(
                    here,
                    back[other][owner, part * span : part * span + LEVEL_TILE, :].astype(f32),
                    tile,
                )
            wanted = (level_row >= 3 * slot) & (level_row < 3 * slot + 3)
            levels.append(jnp.sum(jnp.where(wanted, tile, 0.0), axis=0, keepdims=True))
            pieces.append(piece)
        top = functools.reduce(jnp.maximum, levels)
        weights = [jnp.exp(level - top) for level in levels]
        total = functools.reduce(jnp.add, weights)
        summed = functools.reduce(jnp.add, [w * p for w, p in zip(weights, pieces)])
        memory = summed / total
        stacked = jnp.concatenate([memory[:, :LANES], memory[:, LANES:]], axis=0).T
        upper = stacked[:span]
        lower = stacked[span:]
        first = jnp.where(low, upper, pltpu.roll(lower, head_dim, 1))
        second = jnp.where(low, pltpu.roll(upper, head_dim, 1), lower)
        by_rows = jnp.concatenate([first, second], axis=1)
        start = pl.multiple_of(index * span, span)
        mixed = gated[pl.ds(start, span), :] + gate[pl.ds(start, span), :] * by_rows
        mixed = mixed.astype(bf16)
        side = lax.div(index, half)
        target = pl.multiple_of((index - side * half) * span, span)

        @pl.when(side == core[0])
        def _():
            keep[pl.ds(target, span), :] = mixed

        @pl.when(side != core[0])
        def _():
            send[pl.ds(target, span), :] = mixed

        return carry

    lax.fori_loop(0, spans, one_span, 0)


def output_kernel(core, keep, other, weight, out):
    width = keep.shape[1]
    own = pl.multiple_of(core[0] * width, width)
    far = pl.multiple_of((1 - core[0]) * width, width)
    out[...] = (
        jnp.dot(keep[...], weight[pl.ds(own, width), :], preferred_element_type=f32)
        + jnp.dot(other[...], weight[pl.ds(far, width), :], preferred_element_type=f32)
    ).astype(bf16)


def divisor(count, most):
    return max(size for size in range(1, most + 1) if count % size == 0)


def per_device(
    tokens,
    route_ids,
    store,
    token_gain,
    store_gain,
    carry_weight,
    spatial_weight,
    spatial_gain,
    position_mix,
    position_bias,
    query_weight,
    key_weight,
    read_weight,
    blend_weight,
    output_weight,
):
    row_count, model = tokens.shape
    local_heads, block_length = position_mix.shape[:2]
    width = carry_weight.shape[1]
    head_dim = width // local_heads
    span_count, picks = route_ids.shape
    span = row_count // span_count
    held, length = store.shape[:2]
    owners = lax.axis_size("st")
    cores = lax.axis_size("tp")
    requests = span_count * picks
    capacity = max(1, 2 * requests // owners)
    chunk_count = CHUNKS if capacity % CHUNKS == 0 else 1
    part = capacity // chunk_count
    smem = pl.BlockSpec(memory_space=pltpu.SMEM)
    whole = pl.BlockSpec(memory_space=pltpu.VMEM)
    core = lax.axis_index("tp").astype(jnp.int32).reshape(1)
    flat_ids = route_ids.reshape(requests)

    blocks = 3 if row_count % (3 * 128) == 0 else 1
    token_block = row_count // blocks
    packed = jax.ShapeDtypeStruct((owners, part * span, width), bf16)
    normed, place, *sent = pl.pallas_call(
        functools.partial(
            query_kernel,
            chunk_count=chunk_count,
            capacity=capacity,
            picks=picks,
            span=span,
            held=held,
        ),
        grid=(blocks,),
        in_specs=[
            smem,
            pl.BlockSpec((token_block, model), lambda i: (i, 0)),
            pl.BlockSpec((1, model), lambda i: (0, 0)),
            pl.BlockSpec((model, width), lambda i: (0, 0)),
        ],
        out_specs=[
            pl.BlockSpec((token_block, model), lambda i: (i, 0)),
            smem,
        ]
        + [pl.BlockSpec(packed.shape, lambda i: (0, 0, 0))] * chunk_count,
        out_shape=[
            jax.ShapeDtypeStruct((row_count, model), bf16),
            jax.ShapeDtypeStruct((requests,), jnp.int32),
        ]
        + [packed] * chunk_count,
        scratch_shapes=[
            pltpu.VMEM((row_count, width), bf16),
            pltpu.SMEM((owners,), jnp.int32),
        ],
        compiler_params=params(("arbitrary",)),
        name="queries",
    )(flat_ids, tokens, token_gain.reshape(1, model), query_weight)

    received = [
        lax.all_to_all(piece, "st", split_axis=0, concat_axis=0, tiled=True) for piece in sent
    ]

    all_ids = lax.all_gather(flat_ids, "st", axis=0)
    mine = all_ids // held == lax.axis_index("st")
    order = jnp.arange(requests, dtype=jnp.int32)
    rank = jnp.sum(
        (mine[:, None, :] & (order[None, None, :] < order[None, :, None])).astype(jnp.int32),
        axis=2,
    )
    ranks = jnp.arange(capacity, dtype=jnp.int32)[None, :, None]
    local = jnp.sum(
        jnp.where(mine[:, None, :] & (rank[:, None, :] == ranks), (all_ids % held)[:, None, :], 0),
        axis=2,
    )

    group = divisor(held, 4)
    keys, values = pl.pallas_call(
        store_kernel,
        grid=(held // group,),
        in_specs=[
            pl.BlockSpec((group, length, model), lambda i: (i, 0, 0)),
            pl.BlockSpec((1, model), lambda i: (0, 0)),
            pl.BlockSpec((model, width), lambda i: (0, 0)),
            pl.BlockSpec((model, width), lambda i: (0, 0)),
        ],
        out_specs=[
            pl.BlockSpec((group, length, width), lambda i: (i, 0, 0)),
            pl.BlockSpec((group, width, length), lambda i: (i, 0, 0)),
        ],
        out_shape=[
            jax.ShapeDtypeStruct((held, length, width), bf16),
            jax.ShapeDtypeStruct((held, width, length), bf16),
        ],
        compiler_params=params(("arbitrary",)),
        name="store_rows",
    )(store, store_gain.reshape(1, model), key_weight, read_weight)

    back_rows = part * span + LEVEL_TILE
    owner_group = divisor(owners, 4)
    back = []
    for chunk in range(chunk_count):
        flat_local = local[:, chunk * part : (chunk + 1) * part].reshape(owners * part)
        partial = pl.pallas_call(
            functools.partial(attend_kernel, part=part, span=span, head_dim=head_dim),
            grid=(owners // owner_group,),
            in_specs=[
                smem,
                pl.BlockSpec((owner_group, part * span, width), lambda i: (i, 0, 0)),
                pl.BlockSpec((held, length, width), lambda i: (0, 0, 0)),
                pl.BlockSpec((held, width, length), lambda i: (0, 0, 0)),
            ],
            out_specs=pl.BlockSpec((owner_group, back_rows, width), lambda i: (i, 0, 0)),
            out_shape=jax.ShapeDtypeStruct((owners, back_rows, width), bf16),
            compiler_params=params(("arbitrary",)),
            name="attend",
        )(flat_local, received[chunk], keys, values)
        back.append(lax.all_to_all(partial, "st", split_axis=0, concat_axis=0, tiled=True))

    spatial = jax.nn.gelu(
        jnp.dot(normed, spatial_weight, preferred_element_type=f32), approximate=False
    )
    moments = lax.psum(
        jnp.stack([jnp.sum(spatial, axis=1), jnp.sum(spatial * spatial, axis=1)], axis=1), "tp"
    )
    carry = jax.nn.gelu(
        jnp.dot(normed, carry_weight, preferred_element_type=f32), approximate=False
    )
    gate = jax.nn.sigmoid(jnp.dot(normed, blend_weight, preferred_element_type=f32))
    gated = pl.pallas_call(
        functools.partial(mixing_kernel, head_dim=head_dim, total_width=width * cores),
        grid=(row_count // block_length,),
        in_specs=[
            pl.BlockSpec((block_length, width), lambda i: (i, 0)),
            pl.BlockSpec((block_length, 2), lambda i: (i, 0)),
            pl.BlockSpec((1, width), lambda i: (0, 0)),
            pl.BlockSpec(position_mix.shape, lambda i: (0, 0, 0)),
            pl.BlockSpec((block_length, local_heads), lambda i: (0, 0)),
            pl.BlockSpec((block_length, width), lambda i: (i, 0)),
        ],
        out_specs=pl.BlockSpec((block_length, width), lambda i: (i, 0)),
        out_shape=jax.ShapeDtypeStruct((row_count, width), f32),
        compiler_params=params(("arbitrary",)),
        name="mixing",
    )(spatial, moments, spatial_gain.reshape(1, width), position_mix, position_bias.T, carry)

    half = jax.ShapeDtypeStruct((row_count // cores, width), bf16)
    keep, send = pl.pallas_call(
        functools.partial(
            merge_kernel,
            chunk_count=chunk_count,
            capacity=capacity,
            picks=picks,
            span=span,
            head_dim=head_dim,
        ),
        in_specs=[smem, smem, whole, whole] + [whole] * chunk_count,
        out_specs=[whole, whole],
        out_shape=[half, half],
        compiler_params=params(),
        name="merge",
    )(place, core, gated, gate, *back)
    other = lax.ppermute(send, "tp", [(0, 1), (1, 0)])
    column = model // 4
    return pl.pallas_call(
        output_kernel,
        grid=(4,),
        in_specs=[
            smem,
            pl.BlockSpec(half.shape, lambda i: (0, 0)),
            pl.BlockSpec(half.shape, lambda i: (0, 0)),
            pl.BlockSpec((width * cores, column), lambda i: (0, i)),
        ],
        out_specs=pl.BlockSpec((row_count // cores, column), lambda i: (0, i)),
        out_shape=jax.ShapeDtypeStruct((row_count // cores, model), bf16),
        compiler_params=params(("arbitrary",)),
        name="project",
    )(core, keep, other, output_weight)


def solution(mesh):
    in_specs = (
        P("st", None),
        P("st", None),
        P("st", None, None),
        P(),
        P(),
        P(None, "tp"),
        P(None, "tp"),
        P("tp"),
        P("tp", None, None),
        P("tp", None),
        P(None, "tp"),
        P(None, "tp"),
        P(None, "tp"),
        P(None, "tp"),
        P(),
    )
    out_specs = P(("st", "tp"), None)
    return jax.shard_map(
        per_device, mesh=mesh, in_specs=in_specs, out_specs=out_specs, check_vma=False
    )
```

profile of v0, /device:TPU:13, one launch (start us, length us, event | category | flops | bytes accessed | tf_op | source)
XLA Modules:
  0.0 251.4 jit_solution(1519879528424218435)
XLA Ops:
  0.0 0.9 copy.43
  0.9 0.6 reshape.40.routes
  1.5 8.3 %queries.1 = (bf16[768,2048]{1,0:T(8,128)(2,1)}, s32[48]{0:T(128)}, bf16[16,192,256]{2,1,0:T(8,128)(2,1)}, bf16[16,192,256]{2,1,0:T(8,128)(2,1)}) custom-call(s32[48]{0:T(128)} %reshape.40.routes, bf16[768,2048]{1,0:T(8,128)(2,1)} %tokens.1, f32[1,2048]{1,0:T(1,128)} %bitcast.28, bf16[2048,256]{1,0:T(8,128)(2,1)} %weight.2), custom_call_target="tpu_custom_call" | custom-call | tf_op jit(solution)/shard_map/queries/pallas_call | solution.py:275
  9.8 42.7 %all_to_all.20.queries = bf16[16,192,256]{2,1,0:T(8,128)(2,1)} all-to-all(bf16[16,192,256]{2,1,0:T(8,128)(2,1)} %get-tuple-element.15), channel_id=1, replica_groups=mesh['st'=16,'tp'=2] {'st'}, dimensions={0} | all-to-all | bytes 3145728 | tf_op jit(solution)/shard_map/all_to_all | solution.py:310
  52.4 4.8 %all-to-all-start.2 = ((bf16[16,192,256]{2,1,0:T(8,128)(2,1)}), bf16[16,192,256]{2,1,0:T(8,128)(2,1)S(1)}, u32[]{:S(2)}, u32[]{:S(2)}) async-start(bf16[16,192,256]{2,1,0:T(8,128)(2,1)} %get-tuple-element.18), calls=%async_computation.2 | async-start | bytes 3145728 | tf_op jit(solution)/shard_map/all_to_all | solution.py:310
  57.3 52.1 %all-gather = s32[16,1,48]{2,1,0:T(1,128)S(1)} all-gather(s32[1,1,48]{2,1,0:T(1,128)S(1)} %reshape.46), channel_id=1, replica_groups=mesh['st'=16,'tp'=2] {'st'}, dimensions={0}, use_global_device_ids=true | all-gather | bytes 3264 | tf_op jit(solution)/shard_map/all_gather | solution.py:313
  109.4 0.7 rem.14
  110.1 0.3 convert_reduce_fusion
  110.5 0.2 select_reduce_fusion
  110.7 0.1 copy.52
  110.8 0.6 reshape.43.local
  111.4 13.3 %store_rows.1 = (bf16[24,128,256]{2,1,0:T(8,128)(2,1)}, bf16[24,256,128]{2,1,0:T(8,128)(2,1)}) custom-call(bf16[24,128,2048]{2,1,0:T(8,128)(2,1)} %store.1, f32[1,2048]{1,0:T(1,128)} %bitcast.29, bf16[2048,256]{1,0:T(8,128)(2,1)} %key_weight.1, bf16[2048,256]{1,0:T(8,128)(2,1)} %read_weight.1), custom_call_target="tpu_custom_call" | custom-call | tf_op jit(solution)/shard_map/store_rows/pallas_call | solution.py:327
  124.7 24.5 %attend.2 = bf16[16,208,256]{2,1,0:T(8,128)(2,1)} custom-call(s32[48]{0:T(128)} %reshape.43.local, bf16[16,192,256]{2,1,0:T(8,128)(2,1)} %all_to_all.20.queries, bf16[24,128,256]{2,1,0:T(8,128)(2,1)} %get-tuple-element.16.keys, bf16[24,256,128]{2,1,0:T(8,128)(2,1)} %get-tuple-element.17.values), custom_call_target="tpu_custom_call" | custom-call | tf_op jit(solution)/shard_map/attend/pallas_call | solution.py:353
  149.2 1.2 copy-done.2
  150.4 5.4 %all-to-all-start.1 = ((bf16[16,208,256]{2,1,0:T(8,128)(2,1)}), bf16[16,208,256]{2,1,0:T(8,128)(2,1)S(1)}, u32[]{:S(2)}, u32[]{:S(2)}) async-start(bf16[16,208,256]{2,1,0:T(8,128)(2,1)} %attend.2), calls=%async_computation.1 | async-start | bytes 3407872 | tf_op jit(solution)/shard_map/all_to_all | solution.py:367
  156.0 0.6 reshape.45.local
  156.6 24.4 %attend.3 = bf16[16,208,256]{2,1,0:T(8,128)(2,1)} custom-call(s32[48]{0:T(128)} %reshape.45.local, bf16[16,192,256]{2,1,0:T(8,128)(2,1)} %copy-done.2, bf16[24,128,256]{2,1,0:T(8,128)(2,1)} %get-tuple-element.16.keys, bf16[24,256,128]{2,1,0:T(8,128)(2,1)} %get-tuple-element.17.values), custom_call_target="tpu_custom_call" | custom-call | tf_op jit(solution)/shard_map/attend/pallas_call | solution.py:353
  181.0 12.3 %all-to-all-done.1.rest_0_ = bf16[16,208,256]{2,1,0:T(8,128)(2,1)S(1)} async-done(((bf16[16,208,256]{2,1,0:T(8,128)(2,1)}), bf16[16,208,256]{2,1,0:T(8,128)(2,1)S(1)}, u32[]{:S(2)}, u32[]{:S(2)}) %all-to-all-start.1) | async-done | bytes 1703968 | tf_op jit(solution)/shard_map/all_to_all | solution.py:367
  193.3 4.3 %all-to-all-start.3 = ((bf16[16,208,256]{2,1,0:T(8,128)(2,1)}), bf16[16,208,256]{2,1,0:T(8,128)(2,1)}, u32[]{:S(2)}, u32[]{:S(2)}) async-start(bf16[16,208,256]{2,1,0:T(8,128)(2,1)} %attend.3), calls=%async_computation.3 | async-start | bytes 3407872 | tf_op jit(solution)/shard_map/all_to_all | solution.py:367
  197.6 5.3 %fusion.25 = (f32[768]{0:T(1024)S(1)}, f32[768]{0:T(1024)S(1)}, f32[768,256]{1,0:T(8,128)}) fusion(bf16[768,2048]{1,0:T(8,128)(2,1)} %get-tuple-element.14, bf16[2048,256]{1,0:T(8,128)(2,1)S(1)} %copy-done), kind=kOutput, calls=%fused_computation.54 | convolution fusion | flops 818477568 | bytes 4986880 | tf_op jit(solution)/shard_map/dot_general | solution.py:370
  203.0 0.2 copy.46
  203.2 0.7 copy.47
  203.9 8.9 %psum.7.moments = f32[768,2]{1,0:T(8,128)} all-reduce(f32[768,2]{1,0:T(8,128)S(1)} %copy.46), channel_id=1, replica_groups=mesh['st'=16,'tp'=2] {'tp'}, use_global_device_ids=true, to_apply=%region_2.3 | all-reduce | flops 1536 | bytes 12288 | tf_op jit(solution)/shard_map/psum | solution.py:372
  212.9 5.7 %fusion.6.carry = f32[768,256]{1,0:T(8,128)} fusion(bf16[768,2048]{1,0:T(8,128)(2,1)} %get-tuple-element.14, bf16[2048,256]{1,0:T(8,128)(2,1)} %param.20), kind=kOutput, calls=%fused_computation.9 | convolution fusion | flops 817889280 | bytes 4980736 | tf_op jit(solution)/shard_map/dot_general | solution.py:376
  218.6 5.6 %mixing.1.gated = f32[768,256]{1,0:T(8,128)} custom-call(f32[768,256]{1,0:T(8,128)} %get-tuple-element.23.spatial, f32[768,2]{1,0:T(8,128)} %psum.7.moments, f32[1,256]{1,0:T(1,128)} %bitcast.30, bf16[4,128,128]{2,1,0:T(8,128)(2,1)} %mix.1, f32[128,4]{1,0:T(8,128)} %bitcast.23, f32[768,256]{1,0:T(8,128)} %fusion.6.carry), custom_call_target="tpu_custom_call" | custom-call | tf_op jit(solution)/shard_map/mixing/pallas_call | solution.py:379
  224.1 1.9 fusion.2.gate
  226.0 11.2 %all-to-all-done.3.rest_1_ = bf16[16,208,256]{2,1,0:T(8,128)(2,1)} async-done(((bf16[16,208,256]{2,1,0:T(8,128)(2,1)}), bf16[16,208,256]{2,1,0:T(8,128)(2,1)}, u32[]{:S(2)}, u32[]{:S(2)}) %all-to-all-start.3) | async-done | bytes 1703968 | tf_op jit(solution)/shard_map/all_to_all | solution.py:367
  237.2 6.3 %merge.1 = (bf16[384,256]{1,0:T(8,128)(2,1)}, bf16[384,256]{1,0:T(8,128)(2,1)}) custom-call(s32[48]{0:T(128)} %get-tuple-element.13.place, s32[1]{0:T(128)} %bitcast.core, f32[768,256]{1,0:T(8,128)} %mixing.1.gated, f32[768,256]{1,0:T(8,128)} %fusion.2.gate, bf16[16,208,256]{2,1,0:T(8,128)(2,1)} %copy-done.1, bf16[16,208,256]{2,1,0:T(8,128)(2,1)} %all-to-all-done.3.rest_1_), custom_call_target="tpu_custom_call" | custom-call | tf_op jit(solution)/shard_map/merge/pallas_call | solution.py:397
  243.6 1.4 collective-permute-start
  245.0 1.3 collective-permute-done.other
  246.3 0.7 copy-done.3
  246.9 4.5 %project.1 = bf16[384,2048]{1,0:T(8,128)(2,1)} custom-call(s32[1]{0:T(128)} %bitcast.core, bf16[384,256]{1,0:T(8,128)(2,1)} %get-tuple-element.19.keep, bf16[384,256]{1,0:T(8,128)(2,1)} %copy-done.3, bf16[512,2048]{1,0:T(8,128)(2,1)} %weight.3), custom_call_target="tpu_custom_call" | custom-call | tf_op jit(solution)/shard_map/project/pallas_call | solution.py:414
  (23 shorter events, 0.2 us)
Async XLA Ops:
  0.0 197.6 %copy-start = (bf16[2048,256]{1,0:T(8,128)(2,1)S(1)}, bf16[2048,256]{1,0:T(8,128)(2,1)}, u32[]{:S(2)}) copy-start(bf16[2048,256]{1,0:T(8,128)(2,1)} %param.21) | copy-start | bytes 3145732
  52.4 96.8 %all-to-all-start.2 = ((bf16[16,192,256]{2,1,0:T(8,128)(2,1)}), bf16[16,192,256]{2,1,0:T(8,128)(2,1)S(1)}, u32[]{:S(2)}, u32[]{:S(2)}) async-start(bf16[16,192,256]{2,1,0:T(8,128)(2,1)} %get-tuple-element.18), calls=%async_computation.2 | async-start | bytes 3145728 | tf_op jit(solution)/shard_map/all_to_all | solution.py:310
  149.2 1.3 copy-start.2
  150.4 42.9 %all-to-all-start.1 = ((bf16[16,208,256]{2,1,0:T(8,128)(2,1)}), bf16[16,208,256]{2,1,0:T(8,128)(2,1)S(1)}, u32[]{:S(2)}, u32[]{:S(2)}) async-start(bf16[16,208,256]{2,1,0:T(8,128)(2,1)} %attend.2), calls=%async_computation.1 | async-start | bytes 3407872 | tf_op jit(solution)/shard_map/all_to_all | solution.py:367
  193.3 9.7 %copy-start.1 = (bf16[16,208,256]{2,1,0:T(8,128)(2,1)}, bf16[16,208,256]{2,1,0:T(8,128)(2,1)S(1)}, u32[]{:S(2)}) copy-start(bf16[16,208,256]{2,1,0:T(8,128)(2,1)S(1)} %all-to-all-done.1.rest_0_) | copy-start | bytes 5111812
  193.3 43.9 %all-to-all-start.3 = ((bf16[16,208,256]{2,1,0:T(8,128)(2,1)}), bf16[16,208,256]{2,1,0:T(8,128)(2,1)}, u32[]{:S(2)}, u32[]{:S(2)}) async-start(bf16[16,208,256]{2,1,0:T(8,128)(2,1)} %attend.3), calls=%async_computation.3 | async-start | bytes 3407872 | tf_op jit(solution)/shard_map/all_to_all | solution.py:367
  197.6 5.5 %copy-start.4 = (f32[4,128]{1,0:T(4,128)S(1)}, f32[4,128]{1,0:T(4,128)}, u32[]{:S(2)}) copy-start(f32[4,128]{1,0:T(4,128)} %param.24) | copy-start | bytes 6148
  212.9 11.3 %copy-start.5 = (bf16[768,2048]{1,0:T(8,128)(2,1)S(1)}, bf16[768,2048]{1,0:T(8,128)(2,1)}, u32[]{:S(2)}) copy-start(bf16[768,2048]{1,0:T(8,128)(2,1)} %get-tuple-element.14) | copy-start | bytes 9437188
  212.9 11.3 %copy-start.6 = (bf16[2048,256]{1,0:T(8,128)(2,1)S(1)}, bf16[2048,256]{1,0:T(8,128)(2,1)}, u32[]{:S(2)}) copy-start(bf16[2048,256]{1,0:T(8,128)(2,1)} %param.28) | copy-start | bytes 3145732
  243.6 2.7 %collective-permute-start = (bf16[384,256]{1,0:T(8,128)(2,1)}, bf16[384,256]{1,0:T(8,128)(2,1)S(1)}, u32[]{:S(2)}, u32[]{:S(2)}) collective-permute-start(bf16[384,256]{1,0:T(8,128)(2,1)} %get-tuple-element.20), channel_id=1, source_target_pairs={{0,1},{1,0},{2,3},{3,2},{4,5},{5,4},{6,7},{7,6},{8,9},{9,8},{10,11... | collective-permute-start | bytes 589832 | tf_op jit(solution)/shard_map/ppermute | solution.py:412
  246.3 0.7 copy-start.3
where the time goes:
time: 252 us; the launch traced here: 251 us
  blocking collectives  104 us (41%)
  Pallas kernels  86.9 us (34%)
  waiting for transfers between devices  24.8 us (10%)
  starting transfers between devices  16 us (6%)
  matrix products  12.9 us (5%)
  local copies, waits for them, and re-layouts  5.83 us (2%)
    all_gather x1, blocking collectives, per_device(): all_ids = lax.all_gather(flat_ids, 'st', axis=0)  52.1 us
    pallas_call x2, Pallas kernels, per_device(): pl.pallas_call(functools.partial(attend_kernel, part=part, span=span, hea...  48.9 us
    all_to_all x1, blocking collectives, per_device(): lax.all_to_all(piece, 'st', split_axis=0, concat_axis=0, tiled=True)  42.7 us
    all_to_all x2, waiting for transfers between devices, per_device(): lax.all_to_all(partial, 'st', split_axis=0, concat_axis=0, tiled=True)  23.5 us
    pallas_call x1, Pallas kernels, per_device(): pl.pallas_call(store_kernel, grid=(held // group,), in_specs=[pl.BlockSpe...  13.3 us
    all_to_all x2, starting transfers between devices, per_device(): lax.all_to_all(partial, 'st', split_axis=0, concat_axis=0, tiled=True)  9.77 us
    psum x1, blocking collectives, per_device(): lax.psum(jnp.stack([jnp.sum(spatial, axis=1), jnp.sum(spatial * spatial,...  8.94 us
    pallas_call x1, Pallas kernels, per_device(): pl.pallas_call(functools.partial(query_kernel, chunk_count=chunk_count, c...  8.28 us
  transfers between devices with their start and end apart: 4, of which 3 were waited for; matrix products, arithmetic and copies ran while one was open for 7% of the time, Pallas kernels for 27%

commit v1 on v0

--- a/solution.py
+++ b/solution.py
@@ -28,7 +28,7 @@
 
 
 def query_kernel(
-    routes, tokens, gain, weight, normed, place, *rest, chunk_count, capacity, picks, span, held
+    routes, slots, tokens, gain, weight, normed, place, local, *rest, chunk_count, capacity, picks, span, held
 ):
     sent = rest[:chunk_count]
     queries, counts = rest[chunk_count:]
@@ -47,6 +47,8 @@
 
         def clear(index, carry):
             counts[index] = 0
+            for rank in range(capacity):
+                local[rank, index] = slots[rank, index]
             return carry
 
         lax.fori_loop(0, owners, clear, 0)
@@ -81,7 +83,7 @@
         values[index] = read[index * length : (index + 1) * length].T.astype(bf16)
 
 
-def attend_kernel(local, queries, keys, values, out, *, part, span, head_dim):
+def attend_kernel(local, queries, keys, values, out, *, base, part, span, head_dim):
     owners = queries.shape[0]
     width = queries.shape[2]
     pairs = width // LANES
@@ -94,7 +96,7 @@
     def one_owner(owner, carry):
         levels = [jnp.zeros((LEVEL_TILE, LANES), f32) for _ in range(pairs)]
         for slot in range(part):
-            held = local[(step * owners + owner) * part + slot]
+            held = local[base + slot, step * owners + owner]
             for pair in range(pairs):
                 cut = slice(pair * LANES, (pair + 1) * LANES)
                 piece = queries[owner, slot * span : (slot + 1) * span, cut]
@@ -269,10 +271,22 @@
     core = lax.axis_index("tp").astype(jnp.int32).reshape(1)
     flat_ids = route_ids.reshape(requests)
 
+    all_ids = lax.all_gather(flat_ids, "st", axis=0)
+    mine = all_ids // held == lax.axis_index("st")
+    order = jnp.arange(requests, dtype=jnp.int32)
+    rank = jnp.sum(
+        (mine[:, None, :] & (order[None, None, :] < order[None, :, None])).astype(jnp.int32),
+        axis=2,
+    )
+    ranks = jnp.arange(capacity, dtype=jnp.int32)[:, None, None]
+    local = jnp.sum(
+        jnp.where(mine[None] & (rank[None] == ranks), (all_ids % held)[None], 0), axis=2
+    )
+
     blocks = 3 if row_count % (3 * 128) == 0 else 1
     token_block = row_count // blocks
     packed = jax.ShapeDtypeStruct((owners, part * span, width), bf16)
-    normed, place, *sent = pl.pallas_call(
+    normed, place, local, *sent = pl.pallas_call(
         functools.partial(
             query_kernel,
             chunk_count=chunk_count,
@@ -284,18 +298,21 @@
         grid=(blocks,),
         in_specs=[
             smem,
+            smem,
             pl.BlockSpec((token_block, model), lambda i: (i, 0)),
             pl.BlockSpec((1, model), lambda i: (0, 0)),
             pl.BlockSpec((model, width), lambda i: (0, 0)),
         ],
         out_specs=[
             pl.BlockSpec((token_block, model), lambda i: (i, 0)),
+            smem,
             smem,
         ]
         + [pl.BlockSpec(packed.shape, lambda i: (0, 0, 0))] * chunk_count,
         out_shape=[
             jax.ShapeDtypeStruct((row_count, model), bf16),
             jax.ShapeDtypeStruct((requests,), jnp.int32),
+            jax.ShapeDtypeStruct((capacity, owners), jnp.int32),
         ]
         + [packed] * chunk_count,
         scratch_shapes=[
@@ -304,24 +321,9 @@
         ],
         compiler_params=params(("arbitrary",)),
         name="queries",
-    )(flat_ids, tokens, token_gain.reshape(1, model), query_weight)
-
-    received = [
-        lax.all_to_all(piece, "st", split_axis=0, concat_axis=0, tiled=True) for piece in sent
-    ]
-
-    all_ids = lax.all_gather(flat_ids, "st", axis=0)
-    mine = all_ids // held == lax.axis_index("st")
-    order = jnp.arange(requests, dtype=jnp.int32)
-    rank = jnp.sum(
-        (mine[:, None, :] & (order[None, None, :] < order[None, :, None])).astype(jnp.int32),
-        axis=2,
-    )
-    ranks = jnp.arange(capacity, dtype=jnp.int32)[None, :, None]
-    local = jnp.sum(
-        jnp.where(mine[:, None, :] & (rank[:, None, :] == ranks), (all_ids % held)[:, None, :], 0),
-        axis=2,
-    )
+    )(flat_ids, local, tokens, token_gain.reshape(1, model), query_weight)
+
+    received = [lax.all_to_all(sent[0], "st", split_axis=0, concat_axis=0, tiled=True)]
 
     group = divisor(held, 4)
     keys, values = pl.pallas_call(
@@ -344,27 +346,6 @@
         compiler_params=params(("arbitrary",)),
         name="store_rows",
     )(store, store_gain.reshape(1, model), key_weight, read_weight)
-
-    back_rows = part * span + LEVEL_TILE
-    owner_group = divisor(owners, 4)
-    back = []
-    for chunk in range(chunk_count):
-        flat_local = local[:, chunk * part : (chunk + 1) * part].reshape(owners * part)
-        partial = pl.pallas_call(
-            functools.partial(attend_kernel, part=part, span=span, head_dim=head_dim),
-            grid=(owners // owner_group,),
-            in_specs=[
-                smem,
-                pl.BlockSpec((owner_group, part * span, width), lambda i: (i, 0, 0)),
-                pl.BlockSpec((held, length, width), lambda i: (0, 0, 0)),
-                pl.BlockSpec((held, width, length), lambda i: (0, 0, 0)),
-            ],
-            out_specs=pl.BlockSpec((owner_group, back_rows, width), lambda i: (i, 0, 0)),
-            out_shape=jax.ShapeDtypeStruct((owners, back_rows, width), bf16),
-            compiler_params=params(("arbitrary",)),
-            name="attend",
-        )(flat_local, received[chunk], keys, values)
-        back.append(lax.all_to_all(partial, "st", split_axis=0, concat_axis=0, tiled=True))
 
     spatial = jax.nn.gelu(
         jnp.dot(normed, spatial_weight, preferred_element_type=f32), approximate=False
@@ -392,6 +373,29 @@
         compiler_params=params(("arbitrary",)),
         name="mixing",
     )(spatial, moments, spatial_gain.reshape(1, width), position_mix, position_bias.T, carry)
+
+    for chunk in range(1, chunk_count):
+        received.append(lax.all_to_all(sent[chunk], "st", split_axis=0, concat_axis=0, tiled=True))
+
+    back_rows = part * span + LEVEL_TILE
+    owner_group = divisor(owners, 4)
+    back = []
+    for chunk in range(chunk_count):
+        partial = pl.pallas_call(
+            functools.partial(
+                attend_kernel, base=chunk * part, part=part, span=span, head_dim=head_dim),
+            grid=(owners // owner_group,),
+            in_specs=[
+                smem,
+                pl.BlockSpec((owner_group, part * span, width), lambda i: (i, 0, 0)),
+                pl.BlockSpec((held, length, width), lambda i: (0, 0, 0)),
+                pl.BlockSpec((held, width, length), lambda i: (0, 0, 0)),
+            ],
+            out_specs=pl.BlockSpec((owner_group, back_rows, width), lambda i: (i, 0, 0)),
+            out_shape=jax.ShapeDtypeStruct((owners, back_rows, width), bf16),
+            compiler_params=params(("arbitrary",)),
+        )(local, received[chunk], keys, values)
+        back.append(lax.all_to_all(partial, "st", split_axis=0, concat_axis=0, tiled=True))
 
     half = jax.ShapeDtypeStruct((row_count // cores, width), bf16)
     keep, send = pl.pallas_call(
@@ -446,6 +450,7 @@
         P(),
     )
     out_specs = P(("st", "tp"), None)
+
     return jax.shard_map(
         per_device, mesh=mesh, in_specs=in_specs, out_specs=out_specs, check_vma=False
     )

time: 252 us -> 233 us (0.925)
  blocking collectives: 104 us -> 79 us
  waiting for transfers between devices: 24.8 us -> 30.1 us
    all_gather x1, blocking collectives: 52.1 us -> 23.7 us  [per_device(): all_ids = lax.all_gather(flat_ids, 'st', axis=0)]
    all_to_all x1, blocking collectives: 42.7 us -> 48.5 us  [per_device(): lax.all_to_all(sent[0], 'st', split_axis=0, concat_axis=0, tiled=True)]
    all_to_all x2, waiting for transfers between devices: 23.5 us -> 28.8 us  [per_device(): lax.all_to_all(partial, 'st', split_axis=0, concat_axis=0, tiled=True)]
  transfers between devices with their start and end apart: 4 -> 4, of which waited for: 3 -> 3; matrix products, arithmetic and copies ran while one was open for 7% -> 6% of each run, Pallas kernels for 27% -> 29%
where the time goes in v1:
time: 233 us; the launch traced here: 232 us
  Pallas kernels  87.1 us (37%)
  blocking collectives  79 us (34%)
  waiting for transfers between devices  30.1 us (13%)
  starting transfers between devices  17 us (7%)
  matrix products  12.9 us (6%)
  local copies, waits for them, and re-layouts  4.4 us (2%)
    pallas_call x2, Pallas kernels, per_device(): pl.pallas_call(functools.partial(attend_kernel, base=chunk * part, part=p...  48.9 us
    all_to_all x1, blocking collectives, per_device(): lax.all_to_all(sent[0], 'st', split_axis=0, concat_axis=0, tiled=True)  48.5 us
    all_to_all x2, waiting for transfers between devices, per_device(): lax.all_to_all(partial, 'st', split_axis=0, concat_axis=0, tiled=True)  28.8 us
    all_gather x1, blocking collectives, per_device(): all_ids = lax.all_gather(flat_ids, 'st', axis=0)  23.7 us
    pallas_call x1, Pallas kernels, per_device(): pl.pallas_call(store_kernel, grid=(held // group,), in_specs=[pl.BlockSpe...  13.4 us
    all_to_all x2, starting transfers between devices, per_device(): lax.all_to_all(partial, 'st', split_axis=0, concat_axis=0, tiled=True)  10.7 us
    pallas_call x1, Pallas kernels, per_device(): pl.pallas_call(functools.partial(query_kernel, chunk_count=chunk_count, c...  8.42 us
    psum x1, blocking collectives, per_device(): lax.psum(jnp.stack([jnp.sum(spatial, axis=1), jnp.sum(spatial * spatial,...  6.8 us
  transfers between devices with their start and end apart: 4, of which 3 were waited for; matrix products, arithmetic and copies ran while one was open for 6% of the time, Pallas kernels for 29%

profile of v1, /device:TPU:13, one launch (start us, length us, event | category | flops | bytes accessed | tf_op | source)
XLA Modules:
  0.0 232.4 jit_solution(3260595286198073686)
XLA Ops:
  0.0 0.9 copy.43
  0.9 0.6 reshape.35.routes
  1.5 0.1 reshape.39
  1.6 23.7 %all-gather = s32[16,1,48]{2,1,0:T(1,128)S(1)} all-gather(s32[1,1,48]{2,1,0:T(1,128)S(1)} %reshape.39), channel_id=1, replica_groups=mesh['st'=16,'tp'=2] {'st'}, dimensions={0}, use_global_device_ids=true | all-gather | bytes 3264 | tf_op jit(solution)/shard_map/all_gather | solution.py:274
  25.2 0.7 rem.14
  25.9 0.3 convert_reduce_fusion
  26.3 0.8 select_reduce_fusion.slots
  27.1 8.4 %queries.1 = (bf16[768,2048]{1,0:T(8,128)(2,1)}, s32[48]{0:T(128)}, s32[6,16]{1,0:T(8,128)}, bf16[16,192,256]{2,1,0:T(8,128)(2,1)}, bf16[16,192,256]{2,1,0:T(8,128)(2,1)}) custom-call(s32[48]{0:T(128)} %reshape.35.routes, s32[6,16]{1,0:T(8,128)} %select_reduce_fusion.slots, bf16[768,2048]{1,0:T(8,128)(2,1)} %tokens.1, f32[1,2048]{1,0:T(1,128)} %bitcast.28, ...), custom_call_target="tpu_custom_call" | custom-call | tf_op jit(solution)/shard_map/queries/pallas_call | solution.py:289
  35.5 48.5 %all_to_all.20.queries = bf16[16,192,256]{2,1,0:T(8,128)(2,1)} all-to-all(bf16[16,192,256]{2,1,0:T(8,128)(2,1)} %get-tuple-element.17), channel_id=1, replica_groups=mesh['st'=16,'tp'=2] {'st'}, dimensions={0} | all-to-all | bytes 3145728 | tf_op jit(solution)/shard_map/all_to_all | solution.py:326
  84.0 4.9 %all-to-all-start.2 = ((bf16[16,192,256]{2,1,0:T(8,128)(2,1)}), bf16[16,192,256]{2,1,0:T(8,128)(2,1)S(1)}, u32[]{:S(2)}, u32[]{:S(2)}) async-start(bf16[16,192,256]{2,1,0:T(8,128)(2,1)} %get-tuple-element.20), calls=%async_computation.2 | async-start | bytes 3145728 | tf_op jit(solution)/shard_map/all_to_all | solution.py:378
  88.9 13.4 %store_rows.1 = (bf16[24,128,256]{2,1,0:T(8,128)(2,1)}, bf16[24,256,128]{2,1,0:T(8,128)(2,1)}) custom-call(bf16[24,128,2048]{2,1,0:T(8,128)(2,1)} %store.1, f32[1,2048]{1,0:T(1,128)} %bitcast.29, bf16[2048,256]{1,0:T(8,128)(2,1)} %key_weight.1, bf16[2048,256]{1,0:T(8,128)(2,1)} %read_weight.1), custom_call_target="tpu_custom_call" | custom-call | tf_op jit(solution)/shard_map/store_rows/pallas_call | solution.py:329
  102.3 24.5 %shard_map.145 = bf16[16,208,256]{2,1,0:T(8,128)(2,1)} custom-call(s32[6,16]{1,0:T(8,128)} %get-tuple-element.16.local, bf16[16,192,256]{2,1,0:T(8,128)(2,1)} %all_to_all.20.queries, bf16[24,128,256]{2,1,0:T(8,128)(2,1)} %get-tuple-element.18.keys, bf16[24,256,128]{2,1,0:T(8,128)(2,1)} %get-tuple-element.19.values), custom_call_target="tpu_custom_call" | custom-call | tf_op jit(solution)/shard_map/pallas_call | solution.py:384
  126.7 0.0 all-to-all-done.2.queries
  126.7 1.2 copy-done.2
  128.0 6.4 %all-to-all-start.1 = ((bf16[16,208,256]{2,1,0:T(8,128)(2,1)}), bf16[16,208,256]{2,1,0:T(8,128)(2,1)S(1)}, u32[]{:S(2)}, u32[]{:S(2)}) async-start(bf16[16,208,256]{2,1,0:T(8,128)(2,1)} %shard_map.145), calls=%async_computation.1 | async-start | bytes 3407872 | tf_op jit(solution)/shard_map/all_to_all | solution.py:398
  134.3 24.5 %shard_map.146 = bf16[16,208,256]{2,1,0:T(8,128)(2,1)} custom-call(s32[6,16]{1,0:T(8,128)} %get-tuple-element.16.local, bf16[16,192,256]{2,1,0:T(8,128)(2,1)} %copy-done.2, bf16[24,128,256]{2,1,0:T(8,128)(2,1)} %get-tuple-element.18.keys, bf16[24,256,128]{2,1,0:T(8,128)(2,1)} %get-tuple-element.19.values), custom_call_target="tpu_custom_call" | custom-call | tf_op jit(solution)/shard_map/pallas_call | solution.py:384
  158.8 15.5 %all-to-all-done.1.rest_0_ = bf16[16,208,256]{2,1,0:T(8,128)(2,1)S(1)} async-done(((bf16[16,208,256]{2,1,0:T(8,128)(2,1)}), bf16[16,208,256]{2,1,0:T(8,128)(2,1)S(1)}, u32[]{:S(2)}, u32[]{:S(2)}) %all-to-all-start.1) | async-done | bytes 1703968 | tf_op jit(solution)/shard_map/all_to_all | solution.py:398
  174.3 4.3 %all-to-all-start.3 = ((bf16[16,208,256]{2,1,0:T(8,128)(2,1)}), bf16[16,208,256]{2,1,0:T(8,128)(2,1)}, u32[]{:S(2)}, u32[]{:S(2)}) async-start(bf16[16,208,256]{2,1,0:T(8,128)(2,1)} %shard_map.146), calls=%async_computation.3 | async-start | bytes 3407872 | tf_op jit(solution)/shard_map/all_to_all | solution.py:398
  178.7 0.0 copy-start.4
  178.7 5.3 %fusion.25 = (f32[768]{0:T(1024)S(1)}, f32[768]{0:T(1024)S(1)}, f32[768,256]{1,0:T(8,128)}) fusion(bf16[768,2048]{1,0:T(8,128)(2,1)} %get-tuple-element.15, bf16[2048,256]{1,0:T(8,128)(2,1)S(1)} %copy-done), kind=kOutput, calls=%fused_computation.54 | convolution fusion | flops 818477568 | bytes 4986880 | tf_op jit(solution)/shard_map/dot_general | solution.py:351
  184.0 0.2 copy.50
  184.2 0.7 copy.51
  185.0 6.8 %psum.7.moments = f32[768,2]{1,0:T(8,128)} all-reduce(f32[768,2]{1,0:T(8,128)S(1)} %copy.50), channel_id=1, replica_groups=mesh['st'=16,'tp'=2] {'tp'}, use_global_device_ids=true, to_apply=%region_4.5 | all-reduce | flops 1536 | bytes 12288 | tf_op jit(solution)/shard_map/psum | solution.py:353
  191.8 5.7 %fusion.6.carry = f32[768,256]{1,0:T(8,128)} fusion(bf16[768,2048]{1,0:T(8,128)(2,1)} %get-tuple-element.15, bf16[2048,256]{1,0:T(8,128)(2,1)} %param.20), kind=kOutput, calls=%fused_computation.9 | convolution fusion | flops 817889280 | bytes 4980736 | tf_op jit(solution)/shard_map/dot_general | solution.py:357
  197.5 5.6 %mixing.1.gated = f32[768,256]{1,0:T(8,128)} custom-call(f32[768,256]{1,0:T(8,128)} %get-tuple-element.25.spatial, f32[768,2]{1,0:T(8,128)} %psum.7.moments, f32[1,256]{1,0:T(1,128)} %bitcast.30, bf16[4,128,128]{2,1,0:T(8,128)(2,1)} %mix.1, f32[128,4]{1,0:T(8,128)} %bitcast.23, f32[768,256]{1,0:T(8,128)} %fusion.6.carry), custom_call_target="tpu_custom_call" | custom-call | tf_op jit(solution)/shard_map/mixing/pallas_call | solution.py:360
  203.0 1.9 fusion.2.gate
  204.9 13.3 %all-to-all-done.3.rest_1_ = bf16[16,208,256]{2,1,0:T(8,128)(2,1)} async-done(((bf16[16,208,256]{2,1,0:T(8,128)(2,1)}), bf16[16,208,256]{2,1,0:T(8,128)(2,1)}, u32[]{:S(2)}, u32[]{:S(2)}) %all-to-all-start.3) | async-done | bytes 1703968 | tf_op jit(solution)/shard_map/all_to_all | solution.py:398
  218.2 6.3 %merge.1 = (bf16[384,256]{1,0:T(8,128)(2,1)}, bf16[384,256]{1,0:T(8,128)(2,1)}) custom-call(s32[48]{0:T(128)} %get-tuple-element.14.place, s32[1]{0:T(128)} %bitcast.core, f32[768,256]{1,0:T(8,128)} %mixing.1.gated, f32[768,256]{1,0:T(8,128)} %fusion.2.gate, bf16[16,208,256]{2,1,0:T(8,128)(2,1)} %copy-done.1, bf16[16,208,256]{2,1,0:T(8,128)(2,1)} %all-to-all-done.3.rest_1_), custom_call_target="tpu_custom_call" | custom-call | tf_op jit(solution)/shard_map/merge/pallas_call | solution.py:401
  224.6 1.4 collective-permute-start
  226.0 1.3 collective-permute-done.other
  227.3 0.7 copy-done.3
  227.9 4.5 %project.1 = bf16[384,2048]{1,0:T(8,128)(2,1)} custom-call(s32[1]{0:T(128)} %bitcast.core, bf16[384,256]{1,0:T(8,128)(2,1)} %get-tuple-element.21.keep, bf16[384,256]{1,0:T(8,128)(2,1)} %copy-done.3, bf16[512,2048]{1,0:T(8,128)(2,1)} %weight.3), custom_call_target="tpu_custom_call" | custom-call | tf_op jit(solution)/shard_map/project/pallas_call | solution.py:418
  (18 shorter events, 0.1 us)
Async XLA Ops:
  0.0 178.7 %copy-start = (bf16[2048,256]{1,0:T(8,128)(2,1)S(1)}, bf16[2048,256]{1,0:T(8,128)(2,1)}, u32[]{:S(2)}) copy-start(bf16[2048,256]{1,0:T(8,128)(2,1)} %param.21) | copy-start | bytes 3145732
  84.0 42.7 %all-to-all-start.2 = ((bf16[16,192,256]{2,1,0:T(8,128)(2,1)}), bf16[16,192,256]{2,1,0:T(8,128)(2,1)S(1)}, u32[]{:S(2)}, u32[]{:S(2)}) async-start(bf16[16,192,256]{2,1,0:T(8,128)(2,1)} %get-tuple-element.20), calls=%async_computation.2 | async-start | bytes 3145728 | tf_op jit(solution)/shard_map/all_to_all | solution.py:378
  126.7 1.2 copy-start.2
  128.0 46.3 %all-to-all-start.1 = ((bf16[16,208,256]{2,1,0:T(8,128)(2,1)}), bf16[16,208,256]{2,1,0:T(8,128)(2,1)S(1)}, u32[]{:S(2)}, u32[]{:S(2)}) async-start(bf16[16,208,256]{2,1,0:T(8,128)(2,1)} %shard_map.145), calls=%async_computation.1 | async-start | bytes 3407872 | tf_op jit(solution)/shard_map/all_to_all | solution.py:398
  174.3 9.7 %copy-start.1 = (bf16[16,208,256]{2,1,0:T(8,128)(2,1)}, bf16[16,208,256]{2,1,0:T(8,128)(2,1)S(1)}, u32[]{:S(2)}) copy-start(bf16[16,208,256]{2,1,0:T(8,128)(2,1)S(1)} %all-to-all-done.1.rest_0_) | copy-start | bytes 5111812
  174.3 43.9 %all-to-all-start.3 = ((bf16[16,208,256]{2,1,0:T(8,128)(2,1)}), bf16[16,208,256]{2,1,0:T(8,128)(2,1)}, u32[]{:S(2)}, u32[]{:S(2)}) async-start(bf16[16,208,256]{2,1,0:T(8,128)(2,1)} %shard_map.146), calls=%async_computation.3 | async-start | bytes 3407872 | tf_op jit(solution)/shard_map/all_to_all | solution.py:398
  178.7 5.5 %copy-start.4 = (f32[4,128]{1,0:T(4,128)S(1)}, f32[4,128]{1,0:T(4,128)}, u32[]{:S(2)}) copy-start(f32[4,128]{1,0:T(4,128)} %param.24) | copy-start | bytes 6148
  191.8 11.3 %copy-start.5 = (bf16[768,2048]{1,0:T(8,128)(2,1)S(1)}, bf16[768,2048]{1,0:T(8,128)(2,1)}, u32[]{:S(2)}) copy-start(bf16[768,2048]{1,0:T(8,128)(2,1)} %get-tuple-element.15) | copy-start | bytes 9437188
  191.8 11.3 %copy-start.6 = (bf16[2048,256]{1,0:T(8,128)(2,1)S(1)}, bf16[2048,256]{1,0:T(8,128)(2,1)}, u32[]{:S(2)}) copy-start(bf16[2048,256]{1,0:T(8,128)(2,1)} %param.28) | copy-start | bytes 3145732
  224.6 2.7 %collective-permute-start = (bf16[384,256]{1,0:T(8,128)(2,1)}, bf16[384,256]{1,0:T(8,128)(2,1)S(1)}, u32[]{:S(2)}, u32[]{:S(2)}) collective-permute-start(bf16[384,256]{1,0:T(8,128)(2,1)} %get-tuple-element.22), channel_id=1, source_target_pairs={{0,1},{1,0},{2,3},{3,2},{4,5},{5,4},{6,7},{7,6},{8,9},{9,8},{10,11... | collective-permute-start | bytes 589832 | tf_op jit(solution)/shard_map/ppermute | solution.py:416
  227.3 0.7 copy-start.3

commit v2 on v1

--- a/solution.py
+++ b/solution.py
@@ -28,7 +28,7 @@
 
 
 def query_kernel(
-    routes, slots, tokens, gain, weight, normed, place, local, *rest, chunk_count, capacity, picks, span, held
+    routes, tokens, gain, weight, normed, place, *rest, chunk_count, capacity, picks, span, held
 ):
     sent = rest[:chunk_count]
     queries, counts = rest[chunk_count:]
@@ -47,8 +47,6 @@
 
         def clear(index, carry):
             counts[index] = 0
-            for rank in range(capacity):
-                local[rank, index] = slots[rank, index]
             return carry
 
         lax.fori_loop(0, owners, clear, 0)
@@ -271,7 +269,13 @@
     core = lax.axis_index("tp").astype(jnp.int32).reshape(1)
     flat_ids = route_ids.reshape(requests)
 
-    all_ids = lax.all_gather(flat_ids, "st", axis=0)
+    all_ids = lax.all_to_all(
+        jnp.broadcast_to(flat_ids[None, :], (owners, requests)),
+        "st",
+        split_axis=0,
+        concat_axis=0,
+        tiled=True,
+    )
     mine = all_ids // held == lax.axis_index("st")
     order = jnp.arange(requests, dtype=jnp.int32)
     rank = jnp.sum(
@@ -286,7 +290,7 @@
     blocks = 3 if row_count % (3 * 128) == 0 else 1
     token_block = row_count // blocks
     packed = jax.ShapeDtypeStruct((owners, part * span, width), bf16)
-    normed, place, local, *sent = pl.pallas_call(
+    normed, place, *sent = pl.pallas_call(
         functools.partial(
             query_kernel,
             chunk_count=chunk_count,
@@ -298,21 +302,18 @@
         grid=(blocks,),
         in_specs=[
             smem,
-            smem,
             pl.BlockSpec((token_block, model), lambda i: (i, 0)),
             pl.BlockSpec((1, model), lambda i: (0, 0)),
             pl.BlockSpec((model, width), lambda i: (0, 0)),
         ],
         out_specs=[
             pl.BlockSpec((token_block, model), lambda i: (i, 0)),
-            smem,
             smem,
         ]
         + [pl.BlockSpec(packed.shape, lambda i: (0, 0, 0))] * chunk_count,
         out_shape=[
             jax.ShapeDtypeStruct((row_count, model), bf16),
             jax.ShapeDtypeStruct((requests,), jnp.int32),
-            jax.ShapeDtypeStruct((capacity, owners), jnp.int32),
         ]
         + [packed] * chunk_count,
         scratch_shapes=[
@@ -321,7 +322,7 @@
         ],
         compiler_params=params(("arbitrary",)),
         name="queries",
-    )(flat_ids, local, tokens, token_gain.reshape(1, model), query_weight)
+    )(flat_ids, tokens, token_gain.reshape(1, model), query_weight)
 
     received = [lax.all_to_all(sent[0], "st", split_axis=0, concat_axis=0, tiled=True)]
 

time: 233 us -> 209 us (0.90)
  blocking collectives: 79 us -> 48.8 us
  starting transfers between devices: 17 us -> 23.6 us
    all_gather x1 -> x0, blocking collectives: 23.7 us -> none  [per_device(): all_ids = lax.all_gather(flat_ids, 'st', axis=0)]
    all_to_all x0 -> x1, starting transfers between devices: none -> 6.61 us  [per_device(): lax.all_to_all(jnp.broadcast_to(flat_ids[None, :], (owners, requests)), '...]
    all_to_all x1, blocking collectives: 48.5 us -> 42.4 us  [per_device(): lax.all_to_all(sent[0], 'st', split_axis=0, concat_axis=0, tiled=True)]
  transfers between devices with their start and end apart: 4 -> 5, of which waited for: 3 -> 3; matrix products, arithmetic and copies ran while one was open for 6% -> 7% of each run, Pallas kernels for 29% -> 37%
where the time goes in v2:
time: 209 us; the launch traced here: 208 us
  Pallas kernels  87 us (42%)
  blocking collectives  48.8 us (23%)
  waiting for transfers between devices  30.6 us (15%)
  starting transfers between devices  23.6 us (11%)
  matrix products  12.9 us (6%)
  local copies, waits for them, and re-layouts  4.43 us (2%)
    pallas_call x2, Pallas kernels, per_device(): pl.pallas_call(functools.partial(attend_kernel, base=chunk * part, part=p...  48.9 us
    all_to_all x1, blocking collectives, per_device(): lax.all_to_all(sent[0], 'st', split_axis=0, concat_axis=0, tiled=True)  42.4 us
    all_to_all x2, waiting for transfers between devices, per_device(): lax.all_to_all(partial, 'st', split_axis=0, concat_axis=0, tiled=True)  29.3 us
    pallas_call x1, Pallas kernels, per_device(): pl.pallas_call(store_kernel, grid=(held // group,), in_specs=[pl.BlockSpe...  13.4 us
    all_to_all x2, starting transfers between devices, per_device(): lax.all_to_all(partial, 'st', split_axis=0, concat_axis=0, tiled=True)  10.7 us
    pallas_call x1, Pallas kernels, per_device(): pl.pallas_call(functools.partial(query_kernel, chunk_count=chunk_count, c...  8.32 us
    all_to_all x1, starting transfers between devices, per_device(): lax.all_to_all(jnp.broadcast_to(flat_ids[None, :], (owners, requests)), '...  6.61 us
    psum x1, blocking collectives, per_device(): lax.psum(jnp.stack([jnp.sum(spatial, axis=1), jnp.sum(spatial * spatial,...  6.37 us
  transfers between devices with their start and end apart: 5, of which 3 were waited for; matrix products, arithmetic and copies ran while one was open for 7% of the time, Pallas kernels for 37%

profile of v2, /device:TPU:13, one launch (start us, length us, event | category | flops | bytes accessed | tf_op | source)
XLA Modules:
  0.0 208.5 jit_solution(8298518286183785486)
XLA Ops:
  0.0 0.9 copy.36
  0.9 0.1 reshape.73.routes
  1.0 0.6 broadcast_in_dim.10
  1.6 6.6 %all-to-all-start = ((s32[16,1,48]{2,1,0:T(1,128)}), s32[16,1,48]{2,1,0:T(1,128)S(1)}, u32[]{:S(2)}, u32[]{:S(2)}) async-start(s32[16,1,48]{2,1,0:T(1,128)} %broadcast_in_dim.10), calls=%async_computation | async-start | bytes 16384 | tf_op jit(solution)/shard_map/all_to_all | solution.py:272
  8.2 8.3 %queries.1 = (bf16[768,2048]{1,0:T(8,128)(2,1)}, s32[48]{0:T(128)}, bf16[16,192,256]{2,1,0:T(8,128)(2,1)}, bf16[16,192,256]{2,1,0:T(8,128)(2,1)}) custom-call(s32[48]{0:T(128)} %copy-done.4, bf16[768,2048]{1,0:T(8,128)(2,1)} %tokens.1, f32[1,2048]{1,0:T(1,128)} %bitcast.38, bf16[2048,256]{1,0:T(8,128)(2,1)} %weight.2), custom_call_target="tpu_custom_call" | custom-call | tf_op jit(solution)/shard_map/queries/pallas_call | solution.py:293
  16.5 0.0 all-to-all-done
  16.5 42.4 %all_to_all.26.queries = bf16[16,192,256]{2,1,0:T(8,128)(2,1)} all-to-all(bf16[16,192,256]{2,1,0:T(8,128)(2,1)} %get-tuple-element.15), channel_id=1, replica_groups=mesh['st'=16,'tp'=2] {'st'}, dimensions={0} | all-to-all | bytes 3145728 | tf_op jit(solution)/shard_map/all_to_all | solution.py:327
  58.9 4.9 %all-to-all-start.3 = ((bf16[16,192,256]{2,1,0:T(8,128)(2,1)}), bf16[16,192,256]{2,1,0:T(8,128)(2,1)S(1)}, u32[]{:S(2)}, u32[]{:S(2)}) async-start(bf16[16,192,256]{2,1,0:T(8,128)(2,1)} %get-tuple-element.18), calls=%async_computation.3 | async-start | bytes 3145728 | tf_op jit(solution)/shard_map/all_to_all | solution.py:379
  63.8 13.4 %store_rows.1 = (bf16[24,128,256]{2,1,0:T(8,128)(2,1)}, bf16[24,256,128]{2,1,0:T(8,128)(2,1)}) custom-call(bf16[24,128,2048]{2,1,0:T(8,128)(2,1)} %store.1, f32[1,2048]{1,0:T(1,128)} %bitcast.39, bf16[2048,256]{1,0:T(8,128)(2,1)} %key_weight.1, bf16[2048,256]{1,0:T(8,128)(2,1)} %read_weight.1), custom_call_target="tpu_custom_call" | custom-call | tf_op jit(solution)/shard_map/store_rows/pallas_call | solution.py:330
  77.2 0.3 convert_reduce_fusion
  77.6 0.8 select_reduce_fusion.local
  78.4 24.5 %shard_map.145 = bf16[16,208,256]{2,1,0:T(8,128)(2,1)} custom-call(s32[6,16]{1,0:T(8,128)} %select_reduce_fusion.local, bf16[16,192,256]{2,1,0:T(8,128)(2,1)} %all_to_all.26.queries, bf16[24,128,256]{2,1,0:T(8,128)(2,1)} %get-tuple-element.16.keys, bf16[24,256,128]{2,1,0:T(8,128)(2,1)} %get-tuple-element.17.values), custom_call_target="tpu_custom_call" | custom-call | tf_op jit(solution)/shard_map/pallas_call | solution.py:385
  102.8 0.0 all-to-all-done.3.queries
  102.8 1.2 copy-done.2
  104.1 6.4 %all-to-all-start.2 = ((bf16[16,208,256]{2,1,0:T(8,128)(2,1)}), bf16[16,208,256]{2,1,0:T(8,128)(2,1)S(1)}, u32[]{:S(2)}, u32[]{:S(2)}) async-start(bf16[16,208,256]{2,1,0:T(8,128)(2,1)} %shard_map.145), calls=%async_computation.2 | async-start | bytes 3407872 | tf_op jit(solution)/shard_map/all_to_all | solution.py:399
  110.4 24.5 %shard_map.146 = bf16[16,208,256]{2,1,0:T(8,128)(2,1)} custom-call(s32[6,16]{1,0:T(8,128)} %select_reduce_fusion.local, bf16[16,192,256]{2,1,0:T(8,128)(2,1)} %copy-done.2, bf16[24,128,256]{2,1,0:T(8,128)(2,1)} %get-tuple-element.16.keys, bf16[24,256,128]{2,1,0:T(8,128)(2,1)} %get-tuple-element.17.values), custom_call_target="tpu_custom_call" | custom-call | tf_op jit(solution)/shard_map/pallas_call | solution.py:385
  134.9 15.5 %all-to-all-done.2.rest_0_ = bf16[16,208,256]{2,1,0:T(8,128)(2,1)S(1)} async-done(((bf16[16,208,256]{2,1,0:T(8,128)(2,1)}), bf16[16,208,256]{2,1,0:T(8,128)(2,1)S(1)}, u32[]{:S(2)}, u32[]{:S(2)}) %all-to-all-start.2) | async-done | bytes 1703968 | tf_op jit(solution)/shard_map/all_to_all | solution.py:399
  150.4 4.3 %all-to-all-start.4 = ((bf16[16,208,256]{2,1,0:T(8,128)(2,1)}), bf16[16,208,256]{2,1,0:T(8,128)(2,1)}, u32[]{:S(2)}, u32[]{:S(2)}) async-start(bf16[16,208,256]{2,1,0:T(8,128)(2,1)} %shard_map.146), calls=%async_computation.4 | async-start | bytes 3407872 | tf_op jit(solution)/shard_map/all_to_all | solution.py:399
  154.7 0.0 copy-start.5
  154.7 5.3 %fusion.26 = (f32[768]{0:T(1024)S(1)}, f32[768]{0:T(1024)S(1)}, f32[768,256]{1,0:T(8,128)}) fusion(bf16[768,2048]{1,0:T(8,128)(2,1)} %get-tuple-element.14, bf16[2048,256]{1,0:T(8,128)(2,1)S(1)} %copy-done), kind=kOutput, calls=%fused_computation.59 | convolution fusion | flops 818477568 | bytes 4986880 | tf_op jit(solution)/shard_map/dot_general | solution.py:352
  160.1 0.2 copy.39
  160.3 0.7 copy.40
  161.0 6.4 %psum.7.moments = f32[768,2]{1,0:T(8,128)} all-reduce(f32[768,2]{1,0:T(8,128)S(1)} %copy.39), channel_id=1, replica_groups=mesh['st'=16,'tp'=2] {'tp'}, use_global_device_ids=true, to_apply=%region_2.3 | all-reduce | flops 1536 | bytes 12288 | tf_op jit(solution)/shard_map/psum | solution.py:354
  167.4 5.7 %fusion.6.carry = f32[768,256]{1,0:T(8,128)} fusion(bf16[768,2048]{1,0:T(8,128)(2,1)} %get-tuple-element.14, bf16[2048,256]{1,0:T(8,128)(2,1)} %param.20), kind=kOutput, calls=%fused_computation.9 | convolution fusion | flops 817889280 | bytes 4980736 | tf_op jit(solution)/shard_map/dot_general | solution.py:358
  173.0 5.6 %mixing.1.gated = f32[768,256]{1,0:T(8,128)} custom-call(f32[768,256]{1,0:T(8,128)} %get-tuple-element.23.spatial, f32[768,2]{1,0:T(8,128)} %psum.7.moments, f32[1,256]{1,0:T(1,128)} %bitcast.40, bf16[4,128,128]{2,1,0:T(8,128)(2,1)} %mix.1, f32[128,4]{1,0:T(8,128)} %bitcast.34, f32[768,256]{1,0:T(8,128)} %fusion.6.carry), custom_call_target="tpu_custom_call" | custom-call | tf_op jit(solution)/shard_map/mixing/pallas_call | solution.py:361
  178.6 1.9 fusion.2.gate
  180.5 13.8 %all-to-all-done.4.rest_1_ = bf16[16,208,256]{2,1,0:T(8,128)(2,1)} async-done(((bf16[16,208,256]{2,1,0:T(8,128)(2,1)}), bf16[16,208,256]{2,1,0:T(8,128)(2,1)}, u32[]{:S(2)}, u32[]{:S(2)}) %all-to-all-start.4) | async-done | bytes 1703968 | tf_op jit(solution)/shard_map/all_to_all | solution.py:399
  194.3 6.4 %merge.1 = (bf16[384,256]{1,0:T(8,128)(2,1)}, bf16[384,256]{1,0:T(8,128)(2,1)}) custom-call(s32[48]{0:T(128)} %get-tuple-element.13.place, s32[1]{0:T(128)} %bitcast.core, f32[768,256]{1,0:T(8,128)} %mixing.1.gated, f32[768,256]{1,0:T(8,128)} %fusion.2.gate, bf16[16,208,256]{2,1,0:T(8,128)(2,1)} %copy-done.1, bf16[16,208,256]{2,1,0:T(8,128)(2,1)} %all-to-all-done.4.rest_1_), custom_call_target="tpu_custom_call" | custom-call | tf_op jit(solution)/shard_map/merge/pallas_call | solution.py:402
  200.7 1.4 collective-permute-start
  202.1 1.3 collective-permute-done.other
  203.3 0.7 copy-done.3
  204.0 4.5 %project.1 = bf16[384,2048]{1,0:T(8,128)(2,1)} custom-call(s32[1]{0:T(128)} %bitcast.core, bf16[384,256]{1,0:T(8,128)(2,1)} %get-tuple-element.19.keep, bf16[384,256]{1,0:T(8,128)(2,1)} %copy-done.3, bf16[512,2048]{1,0:T(8,128)(2,1)} %weight.3), custom_call_target="tpu_custom_call" | custom-call | tf_op jit(solution)/shard_map/project/pallas_call | solution.py:419
  (20 shorter events, 0.1 us)
Async XLA Ops:
  0.0 154.7 %copy-start = (bf16[2048,256]{1,0:T(8,128)(2,1)S(1)}, bf16[2048,256]{1,0:T(8,128)(2,1)}, u32[]{:S(2)}) copy-start(bf16[2048,256]{1,0:T(8,128)(2,1)} %param.21) | copy-start | bytes 3145732
  0.9 7.2 %copy-start.4 = (s32[48]{0:T(128)}, s32[48]{0:T(128)S(1)}, u32[]{:S(2)}) copy-start(s32[48]{0:T(128)S(1)} %reshape.73.routes) | copy-start | bytes 580
  1.6 14.9 %all-to-all-start = ((s32[16,1,48]{2,1,0:T(1,128)}), s32[16,1,48]{2,1,0:T(1,128)S(1)}, u32[]{:S(2)}, u32[]{:S(2)}) async-start(s32[16,1,48]{2,1,0:T(1,128)} %broadcast_in_dim.10), calls=%async_computation | async-start | bytes 16384 | tf_op jit(solution)/shard_map/all_to_all | solution.py:272
  58.9 43.9 %all-to-all-start.3 = ((bf16[16,192,256]{2,1,0:T(8,128)(2,1)}), bf16[16,192,256]{2,1,0:T(8,128)(2,1)S(1)}, u32[]{:S(2)}, u32[]{:S(2)}) async-start(bf16[16,192,256]{2,1,0:T(8,128)(2,1)} %get-tuple-element.18), calls=%async_computation.3 | async-start | bytes 3145728 | tf_op jit(solution)/shard_map/all_to_all | solution.py:379
  102.8 1.2 copy-start.2
  104.1 46.3 %all-to-all-start.2 = ((bf16[16,208,256]{2,1,0:T(8,128)(2,1)}), bf16[16,208,256]{2,1,0:T(8,128)(2,1)S(1)}, u32[]{:S(2)}, u32[]{:S(2)}) async-start(bf16[16,208,256]{2,1,0:T(8,128)(2,1)} %shard_map.145), calls=%async_computation.2 | async-start | bytes 3407872 | tf_op jit(solution)/shard_map/all_to_all | solution.py:399
  150.4 9.7 %copy-start.1 = (bf16[16,208,256]{2,1,0:T(8,128)(2,1)}, bf16[16,208,256]{2,1,0:T(8,128)(2,1)S(1)}, u32[]{:S(2)}) copy-start(bf16[16,208,256]{2,1,0:T(8,128)(2,1)S(1)} %all-to-all-done.2.rest_0_) | copy-start | bytes 5111812
  150.4 43.9 %all-to-all-start.4 = ((bf16[16,208,256]{2,1,0:T(8,128)(2,1)}), bf16[16,208,256]{2,1,0:T(8,128)(2,1)}, u32[]{:S(2)}, u32[]{:S(2)}) async-start(bf16[16,208,256]{2,1,0:T(8,128)(2,1)} %shard_map.146), calls=%async_computation.4 | async-start | bytes 3407872 | tf_op jit(solution)/shard_map/all_to_all | solution.py:399
  154.7 5.5 %copy-start.5 = (f32[4,128]{1,0:T(4,128)S(1)}, f32[4,128]{1,0:T(4,128)}, u32[]{:S(2)}) copy-start(f32[4,128]{1,0:T(4,128)} %param.24) | copy-start | bytes 6148
  167.4 11.3 %copy-start.6 = (bf16[768,2048]{1,0:T(8,128)(2,1)S(1)}, bf16[768,2048]{1,0:T(8,128)(2,1)}, u32[]{:S(2)}) copy-start(bf16[768,2048]{1,0:T(8,128)(2,1)} %get-tuple-element.14) | copy-start | bytes 9437188
  167.4 11.3 %copy-start.7 = (bf16[2048,256]{1,0:T(8,128)(2,1)S(1)}, bf16[2048,256]{1,0:T(8,128)(2,1)}, u32[]{:S(2)}) copy-start(bf16[2048,256]{1,0:T(8,128)(2,1)} %param.28) | copy-start | bytes 3145732
  200.7 2.7 %collective-permute-start = (bf16[384,256]{1,0:T(8,128)(2,1)}, bf16[384,256]{1,0:T(8,128)(2,1)S(1)}, u32[]{:S(2)}, u32[]{:S(2)}) collective-permute-start(bf16[384,256]{1,0:T(8,128)(2,1)} %get-tuple-element.20), channel_id=1, source_target_pairs={{0,1},{1,0},{2,3},{3,2},{4,5},{5,4},{6,7},{7,6},{8,9},{9,8},{10,11... | collective-permute-start | bytes 589832 | tf_op jit(solution)/shard_map/ppermute | solution.py:417
  203.3 0.7 copy-start.3
